TPU v7x, 512 devices: a 8x2x16 block of a 8x8x16 slice. The times are simulated.
512 devices in a mesh: grp: 2 (over y), sp: 16 (over z), dp: 16 (over x, core).
Axes of the slice: x: 8, y: 2, z: 16, core: 2. Of those that a mesh axis runs over, the one named last changes fastest.
The devices are a block of a 8x8x16 slice.
Arguments:
- tokens: bfloat16 [32, 2560, 2048], P(('grp', 'dp'), 'sp'), parts along dimension 0, may hold values from -6 to 6
- query_weight: bfloat16 [2048, 1024], P('dp'), may hold values from -0.125 to 0.125
- key_weight: bfloat16 [2048, 256], P('dp'), may hold values from -0.125 to 0.125
- value_weight: bfloat16 [2048, 256], P('dp'), may hold values from -0.125 to 0.125
- out_weight: bfloat16 [1024, 2048], P(None, 'dp'), may hold values from -0.1875 to 0.1875
- query_gain: float32 [64], replicated, may hold values from 0.28 to 6
- key_gain: float32 [64], replicated, may hold values from 0.28 to 6
Outputs:
- mixed: bfloat16 [32, 2560, 2048], P(('grp', 'dp'), 'sp'), parts along dimension 0
There are 2 independent parts, one for each index of `grp`. A program takes and returns all parts, laid end to end along the dimension named above; an argument that names none is the same for every part. Nothing has to cross between parts.
All inputs are finite; a program needn't handle non-finite values.
Results may differ from a plain program's by a relative error of at most 0.006.
The roundings to bfloat16 on the way count: a program that leaves them out, or rounds other values in their place, can miss the bound.
Values may be sent and summed in bfloat16 or wider, within the bound.
A program may use at most 64 MiB of HBM per device.

v0:
```python
import jax
import jax.numpy as jnp
from jax import lax
from jax.sharding import PartitionSpec as P

HEADS = 16
KV_HEADS = 4
HEAD_DIM = 64
GRID_W = 64
theta_base = 10000.0
norm_eps = 1e-06


def sent_together(arrays, axis, dim, along):
    ends, at = ([], 0)
    for a in arrays[:-1]:
        at += a.shape[along]
        ends.append(at)
    both = jnp.concatenate(arrays, axis=along)
    return tuple(jnp.split(lax.all_gather(both, axis, axis=dim, tiled=True), ends, axis=along))


def rotary_tables(positions):
    quarter = HEAD_DIM // 4
    inverse = theta_base ** (-jnp.arange(quarter, dtype=jnp.float32) / quarter)
    grid_rows = (positions // GRID_W).astype(jnp.float32)
    grid_cols = (positions % GRID_W).astype(jnp.float32)
    angles = jnp.concatenate([grid_rows[:, None] * inverse, grid_cols[:, None] * inverse], axis=-1)
    return (jnp.cos(angles), jnp.sin(angles))


def norm_rotate(raw, gain, cosine, sine):
    scaled = raw * lax.rsqrt(jnp.mean(raw * raw, axis=-1, keepdims=True) + norm_eps) * gain
    half = HEAD_DIM // 2
    first_half = scaled[..., :half]
    second_half = scaled[..., half:]
    cosine = cosine[:, None, :]
    sine = sine[:, None, :]
    turned = jnp.concatenate(
        [first_half * cosine - second_half * sine, second_half * cosine + first_half * sine],
        axis=-1,
    )
    return turned.astype(jnp.bfloat16)


def attend_block(queries, keys, values):
    scale = HEAD_DIM ** (-0.5)
    scores = jnp.einsum("qkgd,skd->kgqs", queries, keys, preferred_element_type=jnp.float32) * scale
    top = jnp.max(scores, axis=-1, keepdims=True)
    weights = jnp.exp(scores - top)
    probs = (weights / jnp.sum(weights, axis=-1, keepdims=True)).astype(jnp.bfloat16)
    result = jnp.einsum("kgqs,skd->qkgd", probs, values, preferred_element_type=jnp.float32).astype(
        jnp.bfloat16
    )
    return result.reshape(queries.shape[0], -1)


def shards(tokens, query_weight, key_weight, value_weight, out_weight, query_gain, key_gain):
    tok_rows = tokens.shape[1]
    local_rows = tokens.reshape(tok_rows, tokens.shape[2])
    seq_index = lax.axis_index("sp")
    per_kv = HEADS // KV_HEADS
    pieces = sent_together((query_weight, key_weight, value_weight), "dp", 0, 1)
    raw_q, raw_k, raw_v = tuple(
        (jnp.dot(local_rows, piece, preferred_element_type=jnp.float32) for piece in pieces)
    )
    positions = seq_index * tok_rows + jnp.arange(tok_rows, dtype=jnp.int32)
    cosine, sine = rotary_tables(positions)
    queries = norm_rotate(raw_q.reshape(tok_rows, HEADS, HEAD_DIM), query_gain, cosine, sine)
    keys = norm_rotate(raw_k.reshape(tok_rows, KV_HEADS, HEAD_DIM), key_gain, cosine, sine)
    values = raw_v.astype(jnp.bfloat16).reshape(tok_rows, KV_HEADS, HEAD_DIM)
    kv_pair = jnp.stack(
        [
            keys.reshape(tok_rows, KV_HEADS * HEAD_DIM),
            values.reshape(tok_rows, KV_HEADS * HEAD_DIM),
        ],
        axis=1,
    )
    whole_kv = lax.all_gather(kv_pair, "sp", axis=0, tiled=True)
    length = whole_kv.shape[0]
    all_k = whole_kv[:, 0].reshape(length, KV_HEADS, HEAD_DIM).transpose(1, 0, 2)[:, :, None, :]
    all_v = whole_kv[:, 1].reshape(length, KV_HEADS, HEAD_DIM).transpose(1, 0, 2)[:, :, None, :]
    grouped_q = queries.reshape(tok_rows, KV_HEADS, 1, per_kv, HEAD_DIM).transpose(1, 0, 2, 3, 4)

    def kv_head(operands):
        block_q, block_k, block_v = operands
        return attend_block(block_q, block_k, block_v)

    per_head = lax.map(kv_head, (grouped_q, all_k, all_v))
    attended = per_head.transpose(1, 0, 2).reshape(tok_rows, HEADS * HEAD_DIM)
    result = jnp.dot(
        attended,
        lax.all_gather(out_weight, "dp", axis=1, tiled=True),
        preferred_element_type=jnp.float32,
    )
    return result.astype(jnp.bfloat16).reshape(1, tok_rows, result.shape[1])


def solution(mesh):
    in_specs = (
        P(("grp", "dp"), "sp", None),
        P("dp", None),
        P("dp", None),
        P("dp", None),
        P(None, "dp"),
        P(),
        P(),
    )
    out_specs = P(("grp", "dp"), "sp", None)
    return jax.shard_map(shards, mesh=mesh, in_specs=in_specs, out_specs=out_specs, check_vma=False)
```

profile of v0, /device:TPU:65, one launch (start us, length us, event | category | flops | bytes accessed | tf_op | source)
XLA Modules:
  0.0 242.1 jit_solution(6979037957639061434)
XLA Ops:
  6.6 1.8 pad_maximum_fusion
  8.4 0.1 all-gather.4.cloned.1.call-update
  8.5 0.1 all-gather.6.cloned.1.call-start
  8.6 0.1 broadcast_multiply_fusion.1
  8.7 0.1 fusion.30
  8.8 88.1 %all-gather.4.cloned.1.call-done = bf16[2048,1536]{1,0:T(8,128)(2,1)} async-done(((bf16[128,1536]{1,0:T(8,128)(2,1)}), bf16[2048,1536]{1,0:T(8,128)(2,1)}) %all-gather.4.cloned.1.call-update) | async-done | bytes 6291472 | tf_op jit(solution)/shard_map/all_gather | solution.py:20
  96.9 1.6 convolution_bitcast_fusion
  98.4 0.1 copy.12
  98.6 0.1 multiply_multiply_fusion.1
  98.8 0.1 copy.13
  98.9 1.6 fusion.23
  100.5 0.7 pad_maximum_fusion.1
  101.2 0.1 all-gather.6.cloned.1.call-update
  101.2 0.1 all-gather.8.cloned.1.call-start
  101.3 0.7 all-gather.8.cloned.1.call-update
  102.0 0.1 copy.16
  102.1 0.1 copy.17
  102.2 3.0 %fusion.20 = f32[160,1024]{1,0:T(8,128)S(1)} fusion(bf16[2048,1536]{1,0:T(8,128)(2,1)} %all-gather.4.cloned.1.call-done, bf16[1,160,2048]{2,1,0:T(8,128)(2,1)S(1)} %copy-done), kind=kOutput, calls=%fused_computation.27 | convolution fusion | flops 671088640 | bytes 5505024 | tf_op jit(solution)/shard_map/dot_general | solution.py:65
  105.3 0.3 reshape.204
  105.6 0.4 multiply_reduce_fusion
  106.1 0.4 multiply_multiply_fusion
  106.5 0.6 subtract_convert_fusion
  107.1 0.6 copy.18
  107.7 0.6 copy.19
  108.2 0.9 maximum_bitcast_fusion
  109.1 57.9 %all-gather.6.cloned.1.call-done = bf16[2560,2,256]{2,0,1:T(8,128)(2,1)} async-done(((bf16[160,2,256]{2,0,1:T(8,128)(2,1)}), bf16[2560,2,256]{2,0,1:T(8,128)(2,1)}) %all-gather.6.cloned.1.call-update) | async-done | bytes 2621456 | tf_op jit(solution)/shard_map/all_gather | solution.py:79
  167.0 1.9 fusion.34
  168.9 1.6 copy.14
  170.5 0.7 copy.15
  171.3 27.9 %while.10 = (s32[]{:T(128)}, bf16[4,160,256]{1,2,0:T(8,128)(2,1)}, bf16[4,2560,1,64]{1,3,2,0:T(8,128)(2,1)}, bf16[4,2560,1,64]{1,3,2,0:T(8,128)(2,1)S(1)}, bf16[4,160,1,4,64]{1,4,3,2,0:T(8,128)(2,1)}, /*index=5*/s32[]{:T(128)}) while((s32[]{:T(128)}, bf16[4,160,256]{1,2,0:T(8,128)(2,1)}, bf16[4,2560,1,64]{1,3,2,0:T(8,128)(2,1)}, ...), condition=%wide.region_5.6_spmd, body=%wide.region_2.5_spmd.sunk | while | flops 434215680 | bytes 20757060 | solution.py:89
  171.3 2.1 bitcast_reduce_fusion.2
  173.4 1.2 fusion.43
  174.7 2.9 %fusion.44 = bf16[64,4,160]{2,0,1:T(8,128)(2,1)S(1)} fusion(f32[4,160]{1,0:T(4,128)S(1)} %fusion.43, f32[4,160]{1,0:T(4,128)S(1)} %get-tuple-element.96, f32[2560,160,4]{0,1,2:T(8,128)S(1)} %get-tuple-element.95, bf16[4,2560,1,64]{1,3,2,0:T(8,128)(2,1)} %get-tuple-element.111, s32[]{:T(128)} %get-tuple-element.103), kind=kOutput, calls=%fused_computation.7.clone.1 | convolution fusion | flops 216309760 | bytes 6968832 | tf_op jit(solution)/shard_map/while/body/eval_jaxpr/kgqs,skd->qkgd/dot_general | solution.py:52
  177.6 0.7 constant_dynamic-update-slice_fusion.2
  178.2 2.1 bitcast_reduce_fusion.2
  180.4 1.2 fusion.43
  181.6 2.9 %fusion.44 = bf16[64,4,160]{2,0,1:T(8,128)(2,1)S(1)} fusion(f32[4,160]{1,0:T(4,128)S(1)} %fusion.43, f32[4,160]{1,0:T(4,128)S(1)} %get-tuple-element.96, f32[2560,160,4]{0,1,2:T(8,128)S(1)} %get-tuple-element.95, bf16[4,2560,1,64]{1,3,2,0:T(8,128)(2,1)} %get-tuple-element.111, s32[]{:T(128)} %get-tuple-element.103), kind=kOutput, calls=%fused_computation.7.clone.1 | convolution fusion | flops 216309760 | bytes 6968832 | tf_op jit(solution)/shard_map/while/body/eval_jaxpr/kgqs,skd->qkgd/dot_general | solution.py:52
  184.5 0.7 constant_dynamic-update-slice_fusion.2
  185.2 2.1 bitcast_reduce_fusion.2
  187.3 1.2 fusion.43
  188.6 2.9 %fusion.44 = bf16[64,4,160]{2,0,1:T(8,128)(2,1)S(1)} fusion(f32[4,160]{1,0:T(4,128)S(1)} %fusion.43, f32[4,160]{1,0:T(4,128)S(1)} %get-tuple-element.96, f32[2560,160,4]{0,1,2:T(8,128)S(1)} %get-tuple-element.95, bf16[4,2560,1,64]{1,3,2,0:T(8,128)(2,1)} %get-tuple-element.111, s32[]{:T(128)} %get-tuple-element.103), kind=kOutput, calls=%fused_computation.7.clone.1 | convolution fusion | flops 216309760 | bytes 6968832 | tf_op jit(solution)/shard_map/while/body/eval_jaxpr/kgqs,skd->qkgd/dot_general | solution.py:52
  191.5 0.7 constant_dynamic-update-slice_fusion.2
  192.1 2.2 bitcast_reduce_fusion.2
  194.3 1.2 fusion.43
  195.5 2.9 %fusion.44 = bf16[64,4,160]{2,0,1:T(8,128)(2,1)S(1)} fusion(f32[4,160]{1,0:T(4,128)S(1)} %fusion.43, f32[4,160]{1,0:T(4,128)S(1)} %get-tuple-element.96, f32[2560,160,4]{0,1,2:T(8,128)S(1)} %get-tuple-element.95, bf16[4,2560,1,64]{1,3,2,0:T(8,128)(2,1)} %get-tuple-element.111, s32[]{:T(128)} %get-tuple-element.103), kind=kOutput, calls=%fused_computation.7.clone.1 | convolution fusion | flops 216309760 | bytes 6968832 | tf_op jit(solution)/shard_map/while/body/eval_jaxpr/kgqs,skd->qkgd/dot_general | solution.py:52
  198.5 0.7 constant_dynamic-update-slice_fusion.2
  199.1 32.3 %all-gather.8.cloned.1.call-done = bf16[1024,2048]{1,0:T(8,128)(2,1)} async-done(((bf16[1024,128]{1,0:T(8,128)(2,1)}), bf16[1024,2048]{1,0:T(8,128)(2,1)}) %all-gather.8.cloned.1.call-update) | async-done | bytes 4194320 | tf_op jit(solution)/shard_map/all_gather | solution.py:93
  231.5 4.1 %fusion.19 = bf16[1,160,2048]{2,1,0:T(8,128)(2,1)} fusion(bf16[160,1024]{0,1:T(8,128)(2,1)} %bitcast.109, bf16[1024,2048]{1,0:T(8,128)(2,1)} %all-gather.8.cloned.1.call-done), kind=kOutput, calls=%fused_computation.22 | convolution fusion | flops 671416320 | bytes 5177344 | tf_op jit(solution)/shard_map/dot_general | solution.py:91
  (15 shorter events, 0.2 us)
Async XLA Ops:
  6.5 90.3 %copy-start = (bf16[1,160,2048]{2,1,0:T(8,128)(2,1)S(1)}, bf16[1,160,2048]{2,1,0:T(8,128)(2,1)}, u32[]{:S(2)}) copy-start(bf16[1,160,2048]{2,1,0:T(8,128)(2,1)} %param.9) | copy-start | bytes 1966084
  6.6 92.1 %copy-start.1 = (f32[64]{0:T(128)S(1)}, f32[64]{0:T(128)}, u32[]{:S(2)}) copy-start(f32[64]{0:T(128)} %param.15) | copy-start | bytes 772
  6.6 90.3 %all-gather.4.cloned.1.call-start = ((), (), s32[]{:S(2)}) async-start(), calls=%async_computation | async-start | bytes 6684672 | tf_op jit(solution)/shard_map/all_gather | solution.py:20
  8.5 158.6 %all-gather.6.cloned.1.call-start = ((), (), s32[]{:S(2)}) async-start(), calls=%async_computation.1 | async-start | bytes 2785280 | tf_op jit(solution)/shard_map/all_gather | solution.py:79
  101.2 130.2 %all-gather.8.cloned.1.call-start = ((), (), s32[]{:S(2)}) async-start(), calls=%async_computation.2 | async-start | bytes 4456448 | tf_op jit(solution)/shard_map/all_gather | solution.py:93
  105.3 0.8 copy-start.2
Sparse Core Ops, SparseCore 0:
  9.5 87.3 all-gather.3
  101.4 65.6 all-gather.5
  169.1 62.3 all-gather.7
where the time goes:
time: 243 us; the launch traced here: 242 us
  waiting for transfers between devices  179 us (74%)
  matrix products  30.5 us (13%)
  between operations  13.3 us (5%)
  other arithmetic  10.2 us (4%)
  local copies, waits for them, and re-layouts  8.79 us (4%)
    all_gather x1, waiting for transfers between devices, sent_together(): lax.all_gather(both, axis, axis=dim, tiled=True)  88.1 us
    all_gather x1, waiting for transfers between devices, shards(): whole_kv = lax.all_gather(kv_pair, 'sp', axis=0, tiled=True)  57.9 us
    all_gather x1, waiting for transfers between devices, shards(): lax.all_gather(out_weight, 'dp', axis=1, tiled=True)  32.3 us
    dot_general x4, matrix products, attend_block(): jnp.einsum('kgqs,skd->qkgd', probs, values, preferred_element_type=jnp.fl...  11.6 us
    dot_general x4, matrix products, attend_block(): jnp.einsum('qkgd,skd->kgqs', queries, keys, preferred_element_type=jnp.fl...  8.6 us
    dot_general x3, matrix products, shards(): jnp.dot(local_rows, piece, preferred_element_type=jnp.float32)  6.16 us
    reduce_sum x4, other arithmetic, attend_block(): jnp.sum(weights, axis=-1, keepdims=True)  4.88 us
  transfers between devices with their start and end apart: 3, of which 3 were waited for; matrix products, arithmetic and copies ran while one was open for 16% of the time, Pallas kernels for 0%

commit v1 on v0

--- a/solution.py
+++ b/solution.py
@@ -76,7 +76,24 @@
         ],
         axis=1,
     )
-    whole_kv = lax.all_gather(kv_pair, "sp", axis=0, tiled=True)
+    size, index, span = (lax.axis_size("sp"), lax.axis_index("sp"), kv_pair.shape[0])
+    forward = [(i, (i + 1) % size) for i in range(size)]
+    left = [(i, (i - 1) % size) for i in range(size)]
+    whole = jnp.zeros((*kv_pair.shape[:0], size * span, *kv_pair.shape[0 + 1 :]), kv_pair.dtype)
+    whole = lax.dynamic_update_slice_in_dim(whole, kv_pair, index * span, axis=0)
+    from_left = from_right = kv_pair
+    halfway = size // 2
+    for lap in range(1, halfway + 1):
+        from_left = lax.ppermute(from_left, "sp", forward)
+        whole = lax.dynamic_update_slice_in_dim(
+            whole, from_left, (index - lap) % size * span, axis=0
+        )
+        if lap < size - halfway:
+            from_right = lax.ppermute(from_right, "sp", left)
+            whole = lax.dynamic_update_slice_in_dim(
+                whole, from_right, (index + lap) % size * span, axis=0
+            )
+    whole_kv = whole
     length = whole_kv.shape[0]
     all_k = whole_kv[:, 0].reshape(length, KV_HEADS, HEAD_DIM).transpose(1, 0, 2)[:, :, None, :]
     all_v = whole_kv[:, 1].reshape(length, KV_HEADS, HEAD_DIM).transpose(1, 0, 2)[:, :, None, :]

time: 243 us -> 277 us (1.14)
  the two profiles are of different devices: /device:TPU:65 before, /device:TPU:66 now
where the time goes in v1:
time: 277 us; the launch traced here: 276 us
  waiting for transfers between devices  93.5 us (34%)
  local copies, waits for them, and re-layouts  71.7 us (26%)
  starting transfers between devices  55.1 us (20%)
  matrix products  30.8 us (11%)
  between operations  14.4 us (5%)
  other arithmetic  10.5 us (4%)
    all_gather x1, waiting for transfers between devices, sent_together(): lax.all_gather(both, axis, axis=dim, tiled=True)  86.2 us
    ppermute x7, starting transfers between devices, shards(): from_right = lax.ppermute(from_right, 'sp', left)  37.8 us
    dynamic_update_slice x8, local copies, waits for them, and re-layouts, shards(): lax.dynamic_update_slice_in_dim(whole, from_left, (index - lap) % size *...  22.2 us
    dynamic_update_slice x7, local copies, waits for them, and re-layouts, shards(): lax.dynamic_update_slice_in_dim(whole, from_right, (index + lap) % size *...  21.4 us
    ppermute x8, starting transfers between devices, shards(): from_left = lax.ppermute(from_left, 'sp', forward)  17.2 us
    dot_general x4, matrix products, attend_block(): jnp.einsum('kgqs,skd->qkgd', probs, values, preferred_element_type=jnp.fl...  11.6 us
    dot_general x4, matrix products, attend_block(): jnp.einsum('qkgd,skd->kgqs', queries, keys, preferred_element_type=jnp.fl...  8.94 us
    ppermute x8, local copies, waits for them, and re-layouts, shards(): from_left = lax.ppermute(from_left, 'sp', forward)  8.38 us
  transfers between devices with their start and end apart: 17, of which 9 were waited for; matrix products, arithmetic and copies ran while one was open for 37% of the time, Pallas kernels for 0%

profile of v1, /device:TPU:66, one launch (start us, length us, event | category | flops | bytes accessed | tf_op | source)
XLA Modules:
  0.0 276.0 jit_solution(1793755062558452575)
XLA Ops:
  6.6 1.8 pad_maximum_fusion
  8.8 86.2 %all-gather.3.cloned.1.call-done = bf16[2048,1536]{1,0:T(8,128)(2,1)} async-done(((bf16[128,1536]{1,0:T(8,128)(2,1)}), bf16[2048,1536]{1,0:T(8,128)(2,1)}) %all-gather.3.cloned.1.call-update) | async-done | bytes 6291472 | tf_op jit(solution)/shard_map/all_gather | solution.py:20
  97.1 1.6 fusion.23
  98.7 3.6 %collective-permute-start = (bf16[160,2,256]{2,0,1:T(8,128)(2,1)S(1)}, bf16[160,2,256]{2,0,1:T(8,128)(2,1)S(1)}, u32[]{:S(2)}, u32[]{:S(2)}) collective-permute-start(bf16[160,2,256]{2,0,1:T(8,128)(2,1)S(1)} %pad_maximum_fusion.1), channel_id=1, source_target_pairs={{0,16},{16,32},{32,48},{48,64},{64,80},{80,96},{96,112},{112,128},... | collective-permute-start | bytes 491528 | tf_op jit(solution)/shard_map/ppermute | solution.py:87
  102.3 5.5 %collective-permute-start.1 = (bf16[160,2,256]{2,0,1:T(8,128)(2,1)S(1)}, bf16[160,2,256]{2,0,1:T(8,128)(2,1)S(1)}, u32[]{:S(2)}, u32[]{:S(2)}) collective-permute-start(bf16[160,2,256]{2,0,1:T(8,128)(2,1)S(1)} %pad_maximum_fusion.1), channel_id=1, source_target_pairs={{0,240},{16,0},{32,16},{48,32},{64,48},{80,64},{96,80},{112,96},{1... | collective-permute-start | bytes 491528 | tf_op jit(solution)/shard_map/ppermute | solution.py:92
  107.7 2.6 collective-permute-done
  110.3 1.9 collective-permute-start.2
  113.0 5.2 %collective-permute-start.3 = (bf16[160,2,256]{2,0,1:T(8,128)(2,1)S(1)}, bf16[160,2,256]{2,0,1:T(8,128)(2,1)S(1)}, u32[]{:S(2)}, u32[]{:S(2)}) collective-permute-start(bf16[160,2,256]{2,0,1:T(8,128)(2,1)S(1)} %collective-permute-done.1), channel_id=1, source_target_pairs={{0,240},{16,0},{32,16},{48,32},{64,48},{80,64},{96,80},{112,96},{1... | collective-permute-start | bytes 491528 | tf_op jit(solution)/shard_map/ppermute | solution.py:92
  119.2 1.9 collective-permute-start.4
  121.2 5.5 %collective-permute-start.5 = (bf16[160,2,256]{2,0,1:T(8,128)(2,1)S(1)}, bf16[160,2,256]{2,0,1:T(8,128)(2,1)S(1)}, u32[]{:S(2)}, u32[]{:S(2)}) collective-permute-start(bf16[160,2,256]{2,0,1:T(8,128)(2,1)S(1)} %collective-permute-done.3), channel_id=1, source_target_pairs={{0,240},{16,0},{32,16},{48,32},{64,48},{80,64},{96,80},{112,96},{1... | collective-permute-start | bytes 491528 | tf_op jit(solution)/shard_map/ppermute | solution.py:92
  127.7 1.9 collective-permute-start.6
  130.2 5.2 %collective-permute-start.7 = (bf16[160,2,256]{2,0,1:T(8,128)(2,1)S(1)}, bf16[160,2,256]{2,0,1:T(8,128)(2,1)S(1)}, u32[]{:S(2)}, u32[]{:S(2)}) collective-permute-start(bf16[160,2,256]{2,0,1:T(8,128)(2,1)S(1)} %collective-permute-done.5), channel_id=1, source_target_pairs={{0,240},{16,0},{32,16},{48,32},{64,48},{80,64},{96,80},{112,96},{1... | collective-permute-start | bytes 491528 | tf_op jit(solution)/shard_map/ppermute | solution.py:92
  136.1 1.9 collective-permute-start.8
  138.1 3.0 %fusion.20 = f32[160,1024]{1,0:T(8,128)S(1)} fusion(bf16[2048,1536]{1,0:T(8,128)(2,1)} %all-gather.3.cloned.1.call-done, bf16[1,160,2048]{2,1,0:T(8,128)(2,1)S(1)} %copy-done), kind=kOutput, calls=%fused_computation.27 | convolution fusion | flops 671088640 | bytes 5505024 | tf_op jit(solution)/shard_map/dot_general | solution.py:65
  141.9 5.2 %collective-permute-start.9 = (bf16[160,2,256]{2,0,1:T(8,128)(2,1)S(1)}, bf16[160,2,256]{2,0,1:T(8,128)(2,1)S(1)}, u32[]{:S(2)}, u32[]{:S(2)}) collective-permute-start(bf16[160,2,256]{2,0,1:T(8,128)(2,1)S(1)} %collective-permute-done.7), channel_id=1, source_target_pairs={{0,240},{16,0},{32,16},{48,32},{64,48},{80,64},{96,80},{112,96},{1... | collective-permute-start | bytes 491528 | tf_op jit(solution)/shard_map/ppermute | solution.py:92
  147.1 2.0 collective-permute-start.10
  149.9 5.6 %collective-permute-start.11 = (bf16[160,2,256]{2,0,1:T(8,128)(2,1)S(1)}, bf16[160,2,256]{2,0,1:T(8,128)(2,1)}, u32[]{:S(2)}, u32[]{:S(2)}) collective-permute-start(bf16[160,2,256]{2,0,1:T(8,128)(2,1)S(1)} %collective-permute-done.9), channel_id=1, source_target_pairs={{0,240},{16,0},{32,16},{48,32},{64,48},{80,64},{96,80},{112,96},{1... | collective-permute-start | bytes 491528 | tf_op jit(solution)/shard_map/ppermute | solution.py:92
  155.8 1.9 collective-permute-start.12
  158.4 5.8 %collective-permute-start.13 = (bf16[160,2,256]{2,0,1:T(8,128)(2,1)}, bf16[160,2,256]{2,0,1:T(8,128)(2,1)}, u32[]{:S(2)}, u32[]{:S(2)}) collective-permute-start(bf16[160,2,256]{2,0,1:T(8,128)(2,1)} %collective-permute-done.11), channel_id=1, source_target_pairs={{0,240},{16,0},{32,16},{48,32},{64,48},{80,64},{96,80},{112,96},{1... | collective-permute-start | bytes 491528 | tf_op jit(solution)/shard_map/ppermute | solution.py:92
  164.7 1.9 collective-permute-start.14
  170.1 3.7 %dynamic_update_slice.52 = bf16[2560,2,256]{0,2,1:T(8,128)(2,1)S(1)} dynamic-update-slice(bf16[2560,2,256]{0,2,1:T(8,128)(2,1)S(1)} %broadcast_in_dim.12, bf16[160,2,256]{0,2,1:T(8,128)(2,1)} %copy.28, s32[]{:T(128)S(6)} %select_n.132, s32[]{:T(128)} %copy.72, s32[]{:T(128)} %copy.72) | dynamic-update-slice | bytes 327684 | tf_op jit(solution)/shard_map/dynamic_update_slice | solution.py:83
  173.8 1.8 maximum_bitcast_fusion
  176.7 2.2 dynamic_update_slice.53
  180.0 3.2 %dynamic_update_slice.54 = bf16[2560,2,256]{0,2,1:T(8,128)(2,1)S(1)} dynamic-update-slice(bf16[2560,2,256]{0,2,1:T(8,128)(2,1)S(1)} %dynamic_update_slice.53, bf16[160,2,256]{0,2,1:T(8,128)(2,1)S(1)} %copy.30, s32[]{:T(128)S(6)} %select_n.136, s32[]{:T(128)} %copy.72, s32[]{:T(128)} %copy.72) | dynamic-update-slice | bytes 327684 | tf_op jit(solution)/shard_map/dynamic_update_slice | solution.py:93
  184.2 2.3 dynamic_update_slice.55
  187.6 3.2 %dynamic_update_slice.56 = bf16[2560,2,256]{0,2,1:T(8,128)(2,1)S(1)} dynamic-update-slice(bf16[2560,2,256]{0,2,1:T(8,128)(2,1)S(1)} %dynamic_update_slice.55, bf16[160,2,256]{0,2,1:T(8,128)(2,1)S(1)} %copy.32, s32[]{:T(128)S(6)} %select_n.140, s32[]{:T(128)} %copy.72, s32[]{:T(128)} %copy.72) | dynamic-update-slice | bytes 327684 | tf_op jit(solution)/shard_map/dynamic_update_slice | solution.py:93
  191.8 3.2 %dynamic_update_slice.57 = bf16[2560,2,256]{0,2,1:T(8,128)(2,1)S(1)} dynamic-update-slice(bf16[2560,2,256]{0,2,1:T(8,128)(2,1)S(1)} %dynamic_update_slice.56, bf16[160,2,256]{0,2,1:T(8,128)(2,1)S(1)} %copy.33, s32[]{:T(128)S(6)} %select_n.142, s32[]{:T(128)} %copy.72, s32[]{:T(128)} %copy.72) | dynamic-update-slice | bytes 327684 | tf_op jit(solution)/shard_map/dynamic_update_slice | solution.py:88
  196.1 3.2 %dynamic_update_slice.58 = bf16[2560,2,256]{0,2,1:T(8,128)(2,1)S(1)} dynamic-update-slice(bf16[2560,2,256]{0,2,1:T(8,128)(2,1)S(1)} %dynamic_update_slice.57, bf16[160,2,256]{0,2,1:T(8,128)(2,1)S(1)} %copy.34, s32[]{:T(128)S(6)} %select_n.144, s32[]{:T(128)} %copy.72, s32[]{:T(128)} %copy.72) | dynamic-update-slice | bytes 327684 | tf_op jit(solution)/shard_map/dynamic_update_slice | solution.py:93
  200.3 2.5 dynamic_update_slice.59
  203.8 2.5 dynamic_update_slice.60
  207.4 3.2 %dynamic_update_slice.61 = bf16[2560,2,256]{0,2,1:T(8,128)(2,1)S(1)} dynamic-update-slice(bf16[2560,2,256]{0,2,1:T(8,128)(2,1)S(1)} %dynamic_update_slice.60, bf16[160,2,256]{0,2,1:T(8,128)(2,1)S(1)} %copy.37, s32[]{:T(128)S(6)} %select_n.150, s32[]{:T(128)} %copy.72, s32[]{:T(128)} %copy.72) | dynamic-update-slice | bytes 327684 | tf_op jit(solution)/shard_map/dynamic_update_slice | solution.py:88
  211.6 3.2 %dynamic_update_slice.62 = bf16[2560,2,256]{0,2,1:T(8,128)(2,1)S(1)} dynamic-update-slice(bf16[2560,2,256]{0,2,1:T(8,128)(2,1)S(1)} %dynamic_update_slice.61, bf16[160,2,256]{0,2,1:T(8,128)(2,1)S(1)} %copy.38, s32[]{:T(128)S(6)} %select_n.152, s32[]{:T(128)} %copy.72, s32[]{:T(128)} %copy.72) | dynamic-update-slice | bytes 327684 | tf_op jit(solution)/shard_map/dynamic_update_slice | solution.py:93
  215.8 3.2 %dynamic_update_slice.63 = bf16[2560,2,256]{0,2,1:T(8,128)(2,1)S(1)} dynamic-update-slice(bf16[2560,2,256]{0,2,1:T(8,128)(2,1)S(1)} %dynamic_update_slice.62, bf16[160,2,256]{0,2,1:T(8,128)(2,1)S(1)} %copy.39, s32[]{:T(128)S(6)} %select_n.154, s32[]{:T(128)} %copy.72, s32[]{:T(128)} %copy.72) | dynamic-update-slice | bytes 327684 | tf_op jit(solution)/shard_map/dynamic_update_slice | solution.py:88
  220.0 3.2 %dynamic_update_slice.64 = bf16[2560,2,256]{0,2,1:T(8,128)(2,1)S(1)} dynamic-update-slice(bf16[2560,2,256]{0,2,1:T(8,128)(2,1)S(1)} %dynamic_update_slice.63, bf16[160,2,256]{0,2,1:T(8,128)(2,1)S(1)} %copy.40, s32[]{:T(128)S(6)} %select_n.156, s32[]{:T(128)} %copy.72, s32[]{:T(128)} %copy.72) | dynamic-update-slice | bytes 327684 | tf_op jit(solution)/shard_map/dynamic_update_slice | solution.py:93
  224.3 3.2 %dynamic_update_slice.65 = bf16[2560,2,256]{0,2,1:T(8,128)(2,1)S(1)} dynamic-update-slice(bf16[2560,2,256]{0,2,1:T(8,128)(2,1)S(1)} %dynamic_update_slice.64, bf16[160,2,256]{0,2,1:T(8,128)(2,1)S(1)} %copy.41, s32[]{:T(128)S(6)} %select_n.158, s32[]{:T(128)} %copy.72, s32[]{:T(128)} %copy.72) | dynamic-update-slice | bytes 327684 | tf_op jit(solution)/shard_map/dynamic_update_slice | solution.py:88
  228.5 3.2 %dynamic_update_slice.66 = bf16[2560,2,256]{0,2,1:T(8,128)(2,1)S(1)} dynamic-update-slice(bf16[2560,2,256]{0,2,1:T(8,128)(2,1)S(1)} %dynamic_update_slice.65, bf16[160,2,256]{0,2,1:T(8,128)(2,1)S(1)} %copy.42, s32[]{:T(128)S(6)} %select_n.160, s32[]{:T(128)} %copy.72, s32[]{:T(128)} %copy.72) | dynamic-update-slice | bytes 327684 | tf_op jit(solution)/shard_map/dynamic_update_slice | solution.py:93
  232.7 2.5 dynamic_update_slice.67
  235.2 1.7 fusion.34
  236.9 28.2 %while.10 = (s32[]{:T(128)}, bf16[4,160,256]{1,2,0:T(8,128)(2,1)}, bf16[4,2560,1,64]{1,3,2,0:T(8,128)(2,1)}, bf16[4,2560,1,64]{1,3,2,0:T(8,128)(2,1)}, bf16[4,160,1,4,64]{1,4,3,2,0:T(8,128)(2,1)}, /*index=5*/s32[]{:T(128)}) while((s32[]{:T(128)}, bf16[4,160,256]{1,2,0:T(8,128)(2,1)}, bf16[4,2560,1,64]{1,3,2,0:T(8,128)(2,1)}, ...), condition=%wide.region_5.6_spmd, body=%wide.region_2.5_spmd.sunk | while | flops 434215680 | bytes 20757060 | solution.py:106
  236.9 2.2 bitcast_reduce_fusion.2
  240.3 2.9 %fusion.44 = bf16[64,4,160]{2,0,1:T(8,128)(2,1)S(1)} fusion(f32[4,160]{1,0:T(4,128)S(1)} %fusion.43, f32[4,160]{1,0:T(4,128)S(1)} %get-tuple-element.91, f32[2560,160,4]{0,1,2:T(8,128)S(1)} %get-tuple-element.90, bf16[4,2560,1,64]{1,3,2,0:T(8,128)(2,1)} %get-tuple-element.106, s32[]{:T(128)} %get-tuple-element.98), kind=kOutput, calls=%fused_computation.7.clone.1 | convolution fusion | flops 216309760 | bytes 6968832 | tf_op jit(solution)/shard_map/while/body/eval_jaxpr/kgqs,skd->qkgd/dot_general | solution.py:52
  243.9 2.2 bitcast_reduce_fusion.2
  247.4 2.9 %fusion.44 = bf16[64,4,160]{2,0,1:T(8,128)(2,1)S(1)} fusion(f32[4,160]{1,0:T(4,128)S(1)} %fusion.43, f32[4,160]{1,0:T(4,128)S(1)} %get-tuple-element.91, f32[2560,160,4]{0,1,2:T(8,128)S(1)} %get-tuple-element.90, bf16[4,2560,1,64]{1,3,2,0:T(8,128)(2,1)} %get-tuple-element.106, s32[]{:T(128)} %get-tuple-element.98), kind=kOutput, calls=%fused_computation.7.clone.1 | convolution fusion | flops 216309760 | bytes 6968832 | tf_op jit(solution)/shard_map/while/body/eval_jaxpr/kgqs,skd->qkgd/dot_general | solution.py:52
  251.0 2.2 bitcast_reduce_fusion.2
  254.4 2.9 %fusion.44 = bf16[64,4,160]{2,0,1:T(8,128)(2,1)S(1)} fusion(f32[4,160]{1,0:T(4,128)S(1)} %fusion.43, f32[4,160]{1,0:T(4,128)S(1)} %get-tuple-element.91, f32[2560,160,4]{0,1,2:T(8,128)S(1)} %get-tuple-element.90, bf16[4,2560,1,64]{1,3,2,0:T(8,128)(2,1)} %get-tuple-element.106, s32[]{:T(128)} %get-tuple-element.98), kind=kOutput, calls=%fused_computation.7.clone.1 | convolution fusion | flops 216309760 | bytes 6968832 | tf_op jit(solution)/shard_map/while/body/eval_jaxpr/kgqs,skd->qkgd/dot_general | solution.py:52
  258.0 2.2 bitcast_reduce_fusion.2
  261.5 2.9 %fusion.44 = bf16[64,4,160]{2,0,1:T(8,128)(2,1)S(1)} fusion(f32[4,160]{1,0:T(4,128)S(1)} %fusion.43, f32[4,160]{1,0:T(4,128)S(1)} %get-tuple-element.91, f32[2560,160,4]{0,1,2:T(8,128)S(1)} %get-tuple-element.90, bf16[4,2560,1,64]{1,3,2,0:T(8,128)(2,1)} %get-tuple-element.106, s32[]{:T(128)} %get-tuple-element.98), kind=kOutput, calls=%fused_computation.7.clone.1 | convolution fusion | flops 216309760 | bytes 6968832 | tf_op jit(solution)/shard_map/while/body/eval_jaxpr/kgqs,skd->qkgd/dot_general | solution.py:52
  265.1 4.1 %fusion.19 = bf16[1,160,2048]{2,1,0:T(8,128)(2,1)} fusion(bf16[160,1024]{0,1:T(8,128)(2,1)} %bitcast.105, bf16[1024,2048]{1,0:T(8,128)(2,1)} %all-gather.5.cloned.1.call-done), kind=kOutput, calls=%fused_computation.22 | convolution fusion | flops 671416320 | bytes 5177344 | tf_op jit(solution)/shard_map/dot_general | solution.py:108
  (93 shorter events, 35.7 us)
Async XLA Ops:
  6.5 88.5 %copy-start = (bf16[1,160,2048]{2,1,0:T(8,128)(2,1)S(1)}, bf16[1,160,2048]{2,1,0:T(8,128)(2,1)}, u32[]{:S(2)}) copy-start(bf16[1,160,2048]{2,1,0:T(8,128)(2,1)} %param.9) | copy-start | bytes 1966084
  6.6 90.2 %copy-start.11 = (f32[64]{0:T(128)S(1)}, f32[64]{0:T(128)}, u32[]{:S(2)}) copy-start(f32[64]{0:T(128)} %param.15) | copy-start | bytes 772
  6.6 88.5 %all-gather.3.cloned.1.call-start = ((), (), s32[]{:S(2)}) async-start(), calls=%async_computation | async-start | bytes 6684672 | tf_op jit(solution)/shard_map/all_gather | solution.py:20
  8.5 256.6 %all-gather.5.cloned.1.call-start = ((), (), s32[]{:S(2)}) async-start(), calls=%async_computation.1 | async-start | bytes 4456448 | tf_op jit(solution)/shard_map/all_gather | solution.py:110
  98.7 11.7 %collective-permute-start = (bf16[160,2,256]{2,0,1:T(8,128)(2,1)S(1)}, bf16[160,2,256]{2,0,1:T(8,128)(2,1)S(1)}, u32[]{:S(2)}, u32[]{:S(2)}) collective-permute-start(bf16[160,2,256]{2,0,1:T(8,128)(2,1)S(1)} %pad_maximum_fusion.1), channel_id=1, source_target_pairs={{0,16},{16,32},{32,48},{48,64},{64,80},{80,96},{96,112},{112,128},... | collective-permute-start | bytes 491528 | tf_op jit(solution)/shard_map/ppermute | solution.py:87
  102.3 10.0 %collective-permute-start.1 = (bf16[160,2,256]{2,0,1:T(8,128)(2,1)S(1)}, bf16[160,2,256]{2,0,1:T(8,128)(2,1)S(1)}, u32[]{:S(2)}, u32[]{:S(2)}) collective-permute-start(bf16[160,2,256]{2,0,1:T(8,128)(2,1)S(1)} %pad_maximum_fusion.1), channel_id=1, source_target_pairs={{0,240},{16,0},{32,16},{48,32},{64,48},{80,64},{96,80},{112,96},{1... | collective-permute-start | bytes 491528 | tf_op jit(solution)/shard_map/ppermute | solution.py:92
  110.3 17.3 %copy-start.3 = (bf16[160,2,256]{2,0,1:T(8,128)(2,1)}, bf16[160,2,256]{2,0,1:T(8,128)(2,1)S(1)}, u32[]{:S(2)}) copy-start(bf16[160,2,256]{2,0,1:T(8,128)(2,1)S(1)} %collective-permute-done) | copy-start | bytes 491524
  110.3 8.9 %collective-permute-start.2 = (bf16[160,2,256]{2,0,1:T(8,128)(2,1)S(1)}, bf16[160,2,256]{2,0,1:T(8,128)(2,1)S(1)}, u32[]{:S(2)}, u32[]{:S(2)}) collective-permute-start(bf16[160,2,256]{2,0,1:T(8,128)(2,1)S(1)} %collective-permute-done), channel_id=1, source_target_pairs={{0,16},{16,32},{32,48},{48,64},{64,80},{80,96},{96,112},{112,128},... | collective-permute-start | bytes 491528 | tf_op jit(solution)/shard_map/ppermute | solution.py:87
  112.3 0.7 copy-start.1
  113.0 8.2 %collective-permute-start.3 = (bf16[160,2,256]{2,0,1:T(8,128)(2,1)S(1)}, bf16[160,2,256]{2,0,1:T(8,128)(2,1)S(1)}, u32[]{:S(2)}, u32[]{:S(2)}) collective-permute-start(bf16[160,2,256]{2,0,1:T(8,128)(2,1)S(1)} %collective-permute-done.1), channel_id=1, source_target_pairs={{0,240},{16,0},{32,16},{48,32},{64,48},{80,64},{96,80},{112,96},{1... | collective-permute-start | bytes 491528 | tf_op jit(solution)/shard_map/ppermute | solution.py:92
  119.2 2.0 copy-start.2
  119.2 8.4 %collective-permute-start.4 = (bf16[160,2,256]{2,0,1:T(8,128)(2,1)S(1)}, bf16[160,2,256]{2,0,1:T(8,128)(2,1)S(1)}, u32[]{:S(2)}, u32[]{:S(2)}) collective-permute-start(bf16[160,2,256]{2,0,1:T(8,128)(2,1)S(1)} %collective-permute-done.2), channel_id=1, source_target_pairs={{0,16},{16,32},{32,48},{48,64},{64,80},{80,96},{96,112},{112,128},... | collective-permute-start | bytes 491528 | tf_op jit(solution)/shard_map/ppermute | solution.py:87
  121.2 14.9 %copy-start.4 = (bf16[160,2,256]{2,0,1:T(8,128)(2,1)}, bf16[160,2,256]{2,0,1:T(8,128)(2,1)S(1)}, u32[]{:S(2)}) copy-start(bf16[160,2,256]{2,0,1:T(8,128)(2,1)S(1)} %collective-permute-done.3) | copy-start | bytes 491524
  121.2 9.0 %collective-permute-start.5 = (bf16[160,2,256]{2,0,1:T(8,128)(2,1)S(1)}, bf16[160,2,256]{2,0,1:T(8,128)(2,1)S(1)}, u32[]{:S(2)}, u32[]{:S(2)}) collective-permute-start(bf16[160,2,256]{2,0,1:T(8,128)(2,1)S(1)} %collective-permute-done.3), channel_id=1, source_target_pairs={{0,240},{16,0},{32,16},{48,32},{64,48},{80,64},{96,80},{112,96},{1... | collective-permute-start | bytes 491528 | tf_op jit(solution)/shard_map/ppermute | solution.py:92
  127.7 8.4 %copy-start.5 = (bf16[160,2,256]{2,0,1:T(8,128)(2,1)}, bf16[160,2,256]{2,0,1:T(8,128)(2,1)S(1)}, u32[]{:S(2)}) copy-start(bf16[160,2,256]{2,0,1:T(8,128)(2,1)S(1)} %collective-permute-done.4) | copy-start | bytes 491524
  127.7 8.4 %collective-permute-start.6 = (bf16[160,2,256]{2,0,1:T(8,128)(2,1)S(1)}, bf16[160,2,256]{2,0,1:T(8,128)(2,1)S(1)}, u32[]{:S(2)}, u32[]{:S(2)}) collective-permute-start(bf16[160,2,256]{2,0,1:T(8,128)(2,1)S(1)} %collective-permute-done.4), channel_id=1, source_target_pairs={{0,16},{16,32},{32,48},{48,64},{64,80},{80,96},{96,112},{112,128},... | collective-permute-start | bytes 491528 | tf_op jit(solution)/shard_map/ppermute | solution.py:87
  130.2 10.9 %copy-start.6 = (bf16[160,2,256]{2,0,1:T(8,128)(2,1)}, bf16[160,2,256]{2,0,1:T(8,128)(2,1)S(1)}, u32[]{:S(2)}) copy-start(bf16[160,2,256]{2,0,1:T(8,128)(2,1)S(1)} %collective-permute-done.5) | copy-start | bytes 491524
  130.2 11.7 %collective-permute-start.7 = (bf16[160,2,256]{2,0,1:T(8,128)(2,1)S(1)}, bf16[160,2,256]{2,0,1:T(8,128)(2,1)S(1)}, u32[]{:S(2)}, u32[]{:S(2)}) collective-permute-start(bf16[160,2,256]{2,0,1:T(8,128)(2,1)S(1)} %collective-permute-done.5), channel_id=1, source_target_pairs={{0,240},{16,0},{32,16},{48,32},{64,48},{80,64},{96,80},{112,96},{1... | collective-permute-start | bytes 491528 | tf_op jit(solution)/shard_map/ppermute | solution.py:92
  136.1 5.0 %copy-start.7 = (bf16[160,2,256]{2,0,1:T(8,128)(2,1)}, bf16[160,2,256]{2,0,1:T(8,128)(2,1)S(1)}, u32[]{:S(2)}) copy-start(bf16[160,2,256]{2,0,1:T(8,128)(2,1)S(1)} %collective-permute-done.6) | copy-start | bytes 491524
  136.1 11.0 %collective-permute-start.8 = (bf16[160,2,256]{2,0,1:T(8,128)(2,1)S(1)}, bf16[160,2,256]{2,0,1:T(8,128)(2,1)}, u32[]{:S(2)}, u32[]{:S(2)}) collective-permute-start(bf16[160,2,256]{2,0,1:T(8,128)(2,1)S(1)} %collective-permute-done.6), channel_id=1, source_target_pairs={{0,16},{16,32},{32,48},{48,64},{64,80},{80,96},{96,112},{112,128},... | collective-permute-start | bytes 491528 | tf_op jit(solution)/shard_map/ppermute | solution.py:87
  141.1 16.6 %copy-start.12 = (f32[64]{0:T(128)S(1)}, f32[64]{0:T(128)}, u32[]{:S(2)}) copy-start(f32[64]{0:T(128)} %param.14) | copy-start | bytes 772
  141.9 25.3 %copy-start.8 = (bf16[160,2,256]{2,0,1:T(8,128)(2,1)}, bf16[160,2,256]{2,0,1:T(8,128)(2,1)S(1)}, u32[]{:S(2)}) copy-start(bf16[160,2,256]{2,0,1:T(8,128)(2,1)S(1)} %collective-permute-done.7) | copy-start | bytes 491524
  141.9 8.0 %collective-permute-start.9 = (bf16[160,2,256]{2,0,1:T(8,128)(2,1)S(1)}, bf16[160,2,256]{2,0,1:T(8,128)(2,1)S(1)}, u32[]{:S(2)}, u32[]{:S(2)}) collective-permute-start(bf16[160,2,256]{2,0,1:T(8,128)(2,1)S(1)} %collective-permute-done.7), channel_id=1, source_target_pairs={{0,240},{16,0},{32,16},{48,32},{64,48},{80,64},{96,80},{112,96},{1... | collective-permute-start | bytes 491528 | tf_op jit(solution)/shard_map/ppermute | solution.py:92
  147.1 8.7 %collective-permute-start.10 = (bf16[160,2,256]{2,0,1:T(8,128)(2,1)}, bf16[160,2,256]{2,0,1:T(8,128)(2,1)S(1)}, u32[]{:S(2)}, u32[]{:S(2)}) collective-permute-start(bf16[160,2,256]{2,0,1:T(8,128)(2,1)} %collective-permute-done.8), channel_id=1, source_target_pairs={{0,16},{16,32},{32,48},{48,64},{64,80},{80,96},{96,112},{112,128},... | collective-permute-start | bytes 491528 | tf_op jit(solution)/shard_map/ppermute | solution.py:87
  149.9 17.3 %copy-start.9 = (bf16[160,2,256]{2,0,1:T(8,128)(2,1)}, bf16[160,2,256]{2,0,1:T(8,128)(2,1)S(1)}, u32[]{:S(2)}) copy-start(bf16[160,2,256]{2,0,1:T(8,128)(2,1)S(1)} %collective-permute-done.9) | copy-start | bytes 491524
  149.9 8.4 %collective-permute-start.11 = (bf16[160,2,256]{2,0,1:T(8,128)(2,1)S(1)}, bf16[160,2,256]{2,0,1:T(8,128)(2,1)}, u32[]{:S(2)}, u32[]{:S(2)}) collective-permute-start(bf16[160,2,256]{2,0,1:T(8,128)(2,1)S(1)} %collective-permute-done.9), channel_id=1, source_target_pairs={{0,240},{16,0},{32,16},{48,32},{64,48},{80,64},{96,80},{112,96},{1... | collective-permute-start | bytes 491528 | tf_op jit(solution)/shard_map/ppermute | solution.py:92
  155.8 11.5 %copy-start.10 = (bf16[160,2,256]{2,0,1:T(8,128)(2,1)}, bf16[160,2,256]{2,0,1:T(8,128)(2,1)S(1)}, u32[]{:S(2)}) copy-start(bf16[160,2,256]{2,0,1:T(8,128)(2,1)S(1)} %collective-permute-done.10) | copy-start | bytes 491524
  155.8 8.9 %collective-permute-start.12 = (bf16[160,2,256]{2,0,1:T(8,128)(2,1)S(1)}, bf16[160,2,256]{2,0,1:T(8,128)(2,1)}, u32[]{:S(2)}, u32[]{:S(2)}) collective-permute-start(bf16[160,2,256]{2,0,1:T(8,128)(2,1)S(1)} %collective-permute-done.10), channel_id=1, source_target_pairs={{0,16},{16,32},{32,48},{48,64},{64,80},{80,96},{96,112},{112,128},... | collective-permute-start | bytes 491528 | tf_op jit(solution)/shard_map/ppermute | solution.py:87
  158.4 69.1 %collective-permute-start.13 = (bf16[160,2,256]{2,0,1:T(8,128)(2,1)}, bf16[160,2,256]{2,0,1:T(8,128)(2,1)}, u32[]{:S(2)}, u32[]{:S(2)}) collective-permute-start(bf16[160,2,256]{2,0,1:T(8,128)(2,1)} %collective-permute-done.11), channel_id=1, source_target_pairs={{0,240},{16,0},{32,16},{48,32},{64,48},{80,64},{96,80},{112,96},{1... | collective-permute-start | bytes 491528 | tf_op jit(solution)/shard_map/ppermute | solution.py:92
  164.7 67.0 %collective-permute-start.14 = (bf16[160,2,256]{2,0,1:T(8,128)(2,1)}, bf16[160,2,256]{2,0,1:T(8,128)(2,1)}, u32[]{:S(2)}, u32[]{:S(2)}) collective-permute-start(bf16[160,2,256]{2,0,1:T(8,128)(2,1)} %collective-permute-done.12), channel_id=1, source_target_pairs={{0,16},{16,32},{32,48},{48,64},{64,80},{80,96},{96,112},{112,128},... | collective-permute-start | bytes 491528 | tf_op jit(solution)/shard_map/ppermute | solution.py:87
Sparse Core Ops, SparseCore 0:
  9.5 85.4 all-gather.2
  129.8 52.4 all-gather.4
